TPU v7x, 32 devices: a whole 2x2x4 slice. The times are simulated.
32 devices in a mesh: ep: 8 (over z, core), tp: 4 (over y, x).
Axes of the slice: x: 2, y: 2, z: 4, core: 2. Of those that a mesh axis runs over, the one named last changes fastest.
Arguments:
- mixer_value_input: bfloat16 [2048, 4096], P('ep', 'tp'), may hold values from -6 to 6
- input_state_matrix: bfloat16 [2048, 2048], P('ep', 'tp'), may hold values from -6 to 6
- output_state_matrix: bfloat16 [2048, 2048], P('ep', 'tp'), may hold values from -6 to 6
- output_gate_input: bfloat16 [2048, 4096], P('ep', 'tp'), may hold values from -6 to 6
- step_input: float32 [2048, 64], P('ep', 'tp'), may hold values from -6 to -2
- extra_log_decay: float32 [2048, 64], P('ep', 'tp'), may hold values from -1 to 0
- head_log_decay: float32 [64], P('tp'), may hold values from -10 to 1
- head_skip_scale: float32 [64], P('tp'), may hold values from 0.5 to 2
- value_kernel: float32 [4, 4096], P(None, 'tp'), may hold values from -3 to 3
- input_matrix_kernel: float32 [4, 2048], P(None, 'tp'), may hold values from -3 to 3
- output_matrix_kernel: float32 [4, 2048], P(None, 'tp'), may hold values from -3 to 3
- mixer_norm_scale: float32 [4096], P('tp'), may hold values from 0.1 to 1.9
- mixer_output_weight: bfloat16 [4096, 2048], P(None, 'tp'), may hold values from -0.09375 to 0.09375
- second_token_rows: bfloat16 [2048, 2048], P('ep'), may hold values from -6 to 6
- expert_norm_scale: float32 [2048], replicated, may hold values from 0.1 to 1.9
- routed_expert_index: int32 [2048, 4], P('ep'), may hold values from 0 to 15, all different within a row; in each aligned block of 256 rows (0 to 255, 256 to 511, ...) at most 96 rows name the same one
- routed_expert_weight: float32 [2048, 4], P('ep'), may hold values from 0.1 to 1
- routed_gate_weight: bfloat16 [16, 2048, 1024], P('ep', None, 'tp'), may hold values from -0.125 to 0.125
- routed_up_weight: bfloat16 [16, 2048, 1024], P('ep', None, 'tp'), may hold values from -0.125 to 0.125
- routed_down_weight: bfloat16 [16, 1024, 2048], P('ep', None, 'tp'), may hold values from -0.1875 to 0.1875
- shared_gate_weight: bfloat16 [2048, 1024], P(None, 'tp'), may hold values from -0.125 to 0.125
- shared_up_weight: bfloat16 [2048, 1024], P(None, 'tp'), may hold values from -0.125 to 0.125
- shared_down_weight: bfloat16 [1024, 2048], P(None, 'tp'), may hold values from -0.1875 to 0.1875
Outputs:
- mixer_output: bfloat16 [2048, 2048], P('ep', 'tp')
- routed_out: bfloat16 [2048, 2048], P('ep', 'tp')
Inputs may be any that keep to these rules, and one draw needn't show every extreme that they name: `routed_expert_index`: in each aligned block of 256 rows (the rows of one index of ep) no expert is named more than 96 times, a bound that some block reaches.
All inputs are finite; a program needn't handle non-finite values.
Results may differ from a plain program's by a relative error of at most 0.012.
Values may be sent and summed in bfloat16 or wider, within the bound.
A program may use at most 64 MiB of HBM per device.

v0:
```python
import jax
import jax.numpy as jnp
from jax import lax
from jax.sharding import PartitionSpec as P

HEAD_DIM = 64
STATE = 128
CONV_TAPS = 4
BLOCK = 128
TOP_K = 4
epsilon = 1e-05
precise = lax.Precision.HIGHEST


def passed_along(x, axis, by):
    size = lax.axis_size(axis)
    pairs = [(i, i + by) for i in range(size) if 0 <= i + by < size]
    return lax.ppermute(x, axis, pairs)


def carried_in(total_log, state, axis):
    size = lax.axis_size(axis)
    place = lax.axis_index(axis)
    log = passed_along(total_log, axis, 1)
    hold = passed_along(state.astype(jnp.bfloat16), axis, 1).astype(jnp.float32)
    by = 1
    while by < size - 1:
        before = passed_along(hold.astype(jnp.bfloat16), axis, by).astype(jnp.float32)
        hold = hold + jnp.exp(log)[:, None, None] * before
        log = log + passed_along(log, axis, by)
        by *= 2
    return hold


def conv_silu(tail_rows, source, weights):
    length = source.shape[0]
    padded = jnp.concatenate([tail_rows, source], axis=0)
    total_sum = jnp.zeros(source.shape, jnp.float32)
    for tap_index in range(CONV_TAPS):
        total_sum = (
            total_sum
            + padded[tap_index : tap_index + length].astype(jnp.float32) * weights[tap_index]
        )
    return jax.nn.silu(total_sum).astype(jnp.bfloat16)


def carry_blocks(carried, inputs):
    block_decay, block_state = inputs
    return (carried * block_decay[:, None, None] + block_state, carried)


def earlier_counts(mask, rows):
    at = jnp.arange(rows)
    tri = (at[:, None] < at[None, :]).astype(jnp.bfloat16)
    return lax.dot_general(
        mask.astype(jnp.bfloat16),
        tri,
        (((mask.ndim - 1,), (0,)), ((), ())),
        preferred_element_type=jnp.float32,
    )


def on_device(
    mixer_value_input,
    input_state_matrix,
    output_state_matrix,
    output_gate_input,
    step_input,
    extra_log_decay,
    head_log_decay,
    head_skip_scale,
    value_kernel,
    input_matrix_kernel,
    output_matrix_kernel,
    mixer_norm_scale,
    mixer_output_weight,
    second_token_rows,
    expert_norm_scale,
    routed_expert_index,
    routed_expert_weight,
    routed_gate_weight,
    routed_up_weight,
    routed_down_weight,
    shared_gate_weight,
    shared_up_weight,
    shared_down_weight,
):
    length = mixer_value_input.shape[0]
    heads_local = step_input.shape[1]
    width_x = mixer_value_input.shape[1]
    width_b = input_state_matrix.shape[1]
    groups_local = width_b // STATE
    head_ratio = heads_local // groups_local
    nblocks = length // BLOCK
    lead_row = length - CONV_TAPS + 1
    edge_rows = jnp.concatenate(
        [
            mixer_value_input[lead_row:],
            input_state_matrix[lead_row:],
            output_state_matrix[lead_row:],
        ],
        axis=1,
    )
    tail_rows = passed_along(edge_rows, "ep", 1)
    rows_local = second_token_rows.shape[0]
    model_width = second_token_rows.shape[1]
    local_experts = routed_gate_weight.shape[0]
    ep_count = lax.axis_size("ep")
    experts = local_experts * ep_count
    capacity = max(2, 3 * rows_local * TOP_K // (2 * experts))
    col_width = model_width // lax.axis_size("tp")
    rows_wide = second_token_rows.astype(jnp.float32)
    normed = (
        rows_wide
        * lax.rsqrt(jnp.mean(rows_wide * rows_wide, axis=-1, keepdims=True) + epsilon)
        * expert_norm_scale
    ).astype(jnp.bfloat16)
    ids = routed_expert_index.T.astype(jnp.float32)
    id_rows = -(-ids.size // col_width)
    id_block = jnp.pad(
        ids.astype(jnp.bfloat16).reshape(-1), (0, id_rows * col_width - ids.size)
    ).reshape(id_rows, col_width)
    id_block = jnp.pad(id_block, ((0, -id_rows % 8), (0, 0)))
    my_columns = lax.dynamic_slice_in_dim(normed, lax.axis_index("tp") * col_width, col_width, 1)
    outgoing, value_rows, in_rows, out_rows = lax.optimization_barrier(
        (
            jnp.concatenate([my_columns, id_block], axis=0),
            mixer_value_input,
            input_state_matrix,
            output_state_matrix,
        )
    )
    everyone = lax.all_gather(outgoing, "ep", axis=0)
    values = conv_silu(tail_rows[:, :width_x], value_rows, value_kernel)
    in_mat = conv_silu(tail_rows[:, width_x : width_x + width_b], in_rows, input_matrix_kernel)
    out_mat = conv_silu(tail_rows[:, width_x + width_b :], out_rows, output_matrix_kernel)
    step_length = jax.nn.softplus(step_input)
    decay_logarithm = -jnp.exp(head_log_decay)[None, :] * step_length + extra_log_decay
    running = jnp.cumsum(decay_logarithm.reshape(nblocks, BLOCK, heads_local), axis=1)
    value_wide = values.astype(jnp.float32).reshape(nblocks, BLOCK, heads_local, HEAD_DIM)
    scaled = value_wide * step_length.reshape(nblocks, BLOCK, heads_local)[..., None]
    in_blocks = in_mat.reshape(nblocks, BLOCK, groups_local, STATE)
    out_blocks = out_mat.reshape(nblocks, BLOCK, groups_local, STATE)
    scores = jnp.einsum(
        "bign,bjgn->bgij", out_blocks, in_blocks, preferred_element_type=jnp.float32
    )
    scores = jnp.repeat(scores, head_ratio, axis=1)
    spread = jnp.transpose(running[:, :, None, :] - running[:, None, :, :], (0, 3, 1, 2))
    lower_mask = jnp.tril(jnp.ones((BLOCK, BLOCK), bool))[None, None]
    decay_mat = jnp.where(lower_mask, jnp.exp(jnp.where(lower_mask, spread, 0.0)), 0.0)
    inside = jnp.einsum("bhij,bjhp->bihp", scores * decay_mat, scaled, precision=precise)
    out_head = jnp.repeat(out_blocks.astype(jnp.float32), head_ratio, axis=2)
    in_head = jnp.repeat(in_blocks.astype(jnp.float32), head_ratio, axis=2)
    block_logs = running[:, -1]
    to_end = jnp.exp(block_logs[:, None, :] - running)
    block_state = jnp.einsum("bjhn,bjh,bjhp->bhpn", in_head, to_end, scaled, precision=precise)
    start_state = jnp.zeros((heads_local, HEAD_DIM, STATE), jnp.float32)
    local_total, local_prev = lax.scan(
        carry_blocks, start_state, (jnp.exp(block_logs), block_state)
    )
    before_logs = jnp.cumsum(block_logs, axis=0) - block_logs
    everyone, local_total = lax.optimization_barrier((everyone, local_total))
    incoming = carried_in(jnp.sum(block_logs, axis=0), local_total, "ep")
    their_rows = everyone[:, :rows_local]
    their_ids = everyone[:, rows_local : rows_local + id_rows].reshape(ep_count, -1)
    their_ids = their_ids[:, : ids.size].reshape(ep_count, TOP_K, rows_local).astype(jnp.float32)
    mine = (lax.axis_index("ep") * local_experts + jnp.arange(local_experts)).astype(jnp.float32)
    named = jnp.any(their_ids[:, None] == mine[None, :, None, None], axis=2)
    seat = jnp.where(named, earlier_counts(named, rows_local), -1.0)
    seats = jnp.arange(capacity, dtype=jnp.float32)
    pick = (seat[:, :, None, :] == seats[None, None, :, None]).astype(jnp.bfloat16)
    arrived = jnp.stack(
        [
            jnp.einsum("bsr,brd->bsd", pick[:, j], their_rows, preferred_element_type=jnp.float32)
            .astype(jnp.bfloat16)
            .reshape(ep_count * capacity, col_width)
            for j in range(local_experts)
        ]
    )
    column_piece = lax.all_gather(arrived, "tp", axis=2, tiled=True)
    column_piece, incoming = lax.optimization_barrier((column_piece, incoming))
    entering = local_prev + jnp.exp(before_logs)[:, :, None, None] * incoming[None]
    carried_term = (
        jnp.einsum("bihn,bhpn->bihp", out_head, entering, precision=precise)
        * jnp.exp(running)[..., None]
    )
    mixed_heads = (inside + carried_term).reshape(length, heads_local, HEAD_DIM)
    mixed_heads = mixed_heads + head_skip_scale[None, :, None] * value_wide.reshape(
        length, heads_local, HEAD_DIM
    )
    gated_heads = mixed_heads * jax.nn.silu(output_gate_input.astype(jnp.float32)).reshape(
        length, heads_local, HEAD_DIM
    )
    grouped = gated_heads.reshape(length, groups_local, head_ratio * HEAD_DIM)
    grouped = grouped * lax.rsqrt(jnp.mean(grouped * grouped, axis=-1, keepdims=True) + epsilon)
    mixer_normed = (grouped.reshape(length, width_x) * mixer_norm_scale).astype(jnp.bfloat16)
    gate_pre = jnp.einsum(
        "esd,edf->esf", column_piece, routed_gate_weight, preferred_element_type=jnp.float32
    )
    up_pre = jnp.einsum(
        "esd,edf->esf", column_piece, routed_up_weight, preferred_element_type=jnp.float32
    )
    hidden = (jax.nn.silu(gate_pre) * up_pre).astype(jnp.bfloat16)
    shared_hidden = (
        jax.nn.silu(jnp.dot(normed, shared_gate_weight, preferred_element_type=jnp.float32))
        * jnp.dot(normed, shared_up_weight, preferred_element_type=jnp.float32)
    ).astype(jnp.bfloat16)
    whole_hidden = lax.all_gather(hidden, "tp", axis=2, tiled=True)
    both = lax.all_gather(
        jnp.concatenate([mixer_normed, shared_hidden], axis=1), "tp", axis=1, tiled=True
    ).reshape(length, lax.axis_size("tp"), -1)
    whole_mix = both[:, :, :width_x].reshape(length, -1)
    whole_shared = both[:, :, width_x:].reshape(length, -1)
    mixer_output = jnp.dot(
        whole_mix, mixer_output_weight, preferred_element_type=jnp.float32
    ).astype(jnp.bfloat16)
    expert_result = jnp.einsum(
        "esf,efd->esd", whole_hidden, routed_down_weight, preferred_element_type=jnp.float32
    ).astype(jnp.bfloat16)
    going = jnp.concatenate(
        [expert_result[j].reshape(ep_count, capacity, col_width) for j in range(local_experts)],
        axis=1,
    )
    returned = lax.all_to_all(going, "ep", split_axis=0, concat_axis=0, tiled=True)
    returned = returned.reshape(experts * capacity, col_width)
    kinds = jnp.arange(experts, dtype=jnp.float32)
    chosen = ids[:, None, :] == kinds[None, :, None]
    count = earlier_counts(jnp.any(chosen, axis=0), rows_local)
    position = jnp.sum(jnp.where(chosen, count[None], 0.0), axis=1)
    slot = (ids * capacity + position).T.astype(jnp.int32)
    columns = jnp.arange(experts * capacity, dtype=jnp.int32)[None, :]
    spread = jnp.zeros((rows_local, experts * capacity), jnp.float32)
    for k in range(TOP_K):
        spread = spread + jnp.where(
            slot[:, k : k + 1] == columns, routed_expert_weight[:, k : k + 1], 0.0
        )
    high = lax.reduce_precision(spread, 8, 7)
    low = (spread - high).astype(jnp.bfloat16)
    routed_sum = jnp.dot(
        high.astype(jnp.bfloat16), returned, preferred_element_type=jnp.float32
    ) + jnp.dot(low, returned, preferred_element_type=jnp.float32)
    shared_result = jnp.dot(whole_shared, shared_down_weight, preferred_element_type=jnp.float32)
    routed_out = (routed_sum + shared_result).astype(jnp.bfloat16)
    return (mixer_output, routed_out)


def solution(mesh):
    return jax.shard_map(
        on_device,
        mesh=mesh,
        in_specs=(
            P("ep", "tp"),
            P("ep", "tp"),
            P("ep", "tp"),
            P("ep", "tp"),
            P("ep", "tp"),
            P("ep", "tp"),
            P("tp"),
            P("tp"),
            P(None, "tp"),
            P(None, "tp"),
            P(None, "tp"),
            P("tp"),
            P(None, "tp"),
            P("ep", None),
            P(),
            P("ep", None),
            P("ep", None),
            P("ep", None, "tp"),
            P("ep", None, "tp"),
            P("ep", None, "tp"),
            P(None, "tp"),
            P(None, "tp"),
            P(None, "tp"),
        ),
        out_specs=(P("ep", "tp"), P("ep", "tp")),
        check_vma=False,
    )
```

profile of v0, /device:TPU:0, one launch (start us, length us, event | category | flops | bytes accessed | tf_op | source)
XLA Modules:
  0.0 239.8 jit_solution(12581473368572431942)
XLA Ops:
  10.7 3.2 %collective-permute-start = (bf16[3,2048]{0,1:T(8,128)(2,1)}, bf16[3,2048]{0,1:T(8,128)(2,1)}, u32[]{:S(2)}, u32[]{:S(2)}) collective-permute-start(bf16[3,2048]{0,1:T(8,128)(2,1)} %copy.77), channel_id=1, source_target_pairs={{0,4},{4,8},{8,12},{12,16},{16,20},{20,24},{24,28},{1,5},{5,9},{9,... | collective-permute-start | bytes 36872 | tf_op jit(solution)/shard_map/ppermute | solution.py:18
  26.7 3.4 %multiply_convert_fusion.2 = (bf16[256,512]{1,0:T(8,128)(2,1)}, bf16[256,512]{1,0:T(8,128)(2,1)}) fusion(bf16[256,512]{1,0:T(8,128)(2,1)} %param.26, bf16[3,512]{1,0:T(4,128)(2,1)} %copy.81, f32[512]{0:T(512)} %bitcast.141, f32[512]{0:T(512)} %bitcast.142, f32[512]{0:T(512)} %bitcast.140, f32[512]{0:T(512)} %bitcast.139, f32[512]{0:T(512)} %bitcast.145, ...), kind=kLoop, calls=%fused_computation.103 | loop fusion | flops 6553600 | bytes 1071104 | tf_op jit(solution)/shard_map/convert_element_type | solution.py:44
  32.9 2.9 %fusion.71 = f32[256,1024]{0,1:T(8,128)} fusion(f32[1024]{0:T(1024)} %bitcast.134, bf16[256,1024]{0,1:T(8,128)(2,1)S(1)} %copy.78, f32[1024]{0:T(1024)} %bitcast.135, bf16[3,1024]{0,1:T(8,128)(2,1)S(1)} %slice.176, f32[1024]{0:T(1024)} %bitcast.133, f32[1024]{0:T(1024)} %bitcast.132), kind=kLoop, calls=%fused_computation.106 | loop fusion | flops 6815744 | bytes 1595392 | tf_op jit(solution)/shard_map/convert_element_type | solution.py:140
  35.8 2.7 %reshape.132 = f32[2,128,16,64]{1,0,3,2:T(2,128)} reshape(f32[256,1024]{0,1:T(8,128)} %fusion.71) | data formatting | bytes 2097152 | tf_op jit(solution)/shard_map/reshape | solution.py:140
  38.6 3.0 %broadcast_multiply_fusion = (f32[2,128,16,64]{1,0,3,2:T(2,128)S(1)}, f32[2,128,16,64]{1,0,3,2:T(2,128)}) fusion(f32[2,128,16]{1,0,2:T(2,128)S(1)} %copy.88, f32[2,128,16,64]{1,0,3,2:T(2,128)} %reshape.132, f32[2,128,16]{1,0,2:T(2,128)} %mul.326), kind=kLoop, calls=%fused_computation.102 | loop fusion | flops 524288 | bytes 3178496 | tf_op jit(solution)/shard_map/bjhn,bjh,bjhp->bhpn/dot_general | solution.py:156
  41.8 3.1 %fusion.37 = f32[2,16,64,128]{3,2,1,0:T(8,128)} fusion(f32[2,128,16,128]{3,1,2,0:T(8,128)S(1)} %bitcast.120, f32[2,128,16,64]{1,0,3,2:T(2,128)S(1)} %get-tuple-element.78), kind=kOutput, calls=%fused_computation.55 | convolution fusion | flops 402653184 | bytes 4194304 | tf_op jit(solution)/shard_map/bjhn,bjh,bjhp->bhpn/dot_general | solution.py:156
  44.9 4.0 %while.13 = (s32[]{:T(128)}, f32[16,64,128]{2,1,0:T(8,128)S(1)}, f32[2,16,64,128]{3,2,1,0:T(8,128)}, f32[2,16]{1,0:T(2,128)S(1)}, f32[2,16,64,128]{3,2,1,0:T(8,128)}, /*index=5*/s32[]{:T(128)}, s32[]{:T(128)}) while((s32[]{:T(128)}, f32[16,64,128]{2,1,0:T(8,128)S(1)}, f32[2,16,64,128]{3,2,1,0:T(8,128)}, f32[2,16]{1,0:T(2,128)S(1)}, ...), condition=%wide.region_3.4_spmd.clone, body=%wide.region_2.3_spmd.clone.sunk | while | flops 524291 | bytes 2621740 | solution.py:158
  51.3 2.3 fusion.18
  55.5 3.0 %collective-permute-start.1 = (bf16[16,64,128]{2,1,0:T(8,128)(2,1)S(1)}, bf16[16,64,128]{2,1,0:T(8,128)(2,1)S(1)}, u32[]{:S(2)}, u32[]{:S(2)}) collective-permute-start(bf16[16,64,128]{2,1,0:T(8,128)(2,1)S(1)} %convert_element_type.179), channel_id=1, source_target_pairs={{0,4},{4,8},{8,12},{12,16},{16,20},{20,24},{24,28},{1,5},{5,9},{9,... | collective-permute-start | bytes 786440 | tf_op jit(solution)/shard_map/ppermute | solution.py:18
  59.7 4.5 %collective-permute-start.3 = (bf16[16,64,128]{2,1,0:T(8,128)(2,1)S(1)}, bf16[16,64,128]{2,1,0:T(8,128)(2,1)S(1)}, u32[]{:S(2)}, u32[]{:S(2)}) collective-permute-start(bf16[16,64,128]{2,1,0:T(8,128)(2,1)S(1)} %collective-permute-done.1), channel_id=1, source_target_pairs={{0,4},{4,8},{8,12},{12,16},{16,20},{20,24},{24,28},{1,5},{5,9},{9,... | collective-permute-start | bytes 786440 | tf_op jit(solution)/shard_map/ppermute | solution.py:18
  64.2 4.4 %collective-permute-start.2 = (f32[16]{0:T(128)S(1)}, f32[16]{0:T(128)S(1)}, u32[]{:S(2)}, u32[]{:S(2)}) collective-permute-start(f32[16]{0:T(128)S(1)} %copy-done.31), channel_id=1, source_target_pairs={{0,4},{4,8},{8,12},{12,16},{16,20},{20,24},{24,28},{1,5},{5,9},{9,... | collective-permute-start | bytes 200 | tf_op jit(solution)/shard_map/ppermute | solution.py:18
  69.4 2.5 %collective-permute-start.4 = (f32[16]{0:T(128)S(1)}, f32[16]{0:T(128)S(1)}, u32[]{:S(2)}, u32[]{:S(2)}) collective-permute-start(f32[16]{0:T(128)S(1)} %collective-permute-done.2), channel_id=1, source_target_pairs={{0,4},{4,8},{8,12},{12,16},{16,20},{20,24},{24,28},{1,5},{5,9},{9,... | collective-permute-start | bytes 200 | tf_op jit(solution)/shard_map/ppermute | solution.py:18
  72.9 6.5 %collective-permute-start.5 = (bf16[16,64,128]{2,1,0:T(8,128)(2,1)S(1)}, bf16[16,64,128]{2,1,0:T(8,128)(2,1)S(1)}, u32[]{:S(2)}, u32[]{:S(2)}) collective-permute-start(bf16[16,64,128]{2,1,0:T(8,128)(2,1)S(1)} %fusion.72), channel_id=1, source_target_pairs={{0,8},{4,12},{8,16},{12,20},{16,24},{20,28},{1,9},{5,13},{9,17},{1... | collective-permute-start | bytes 786440 | tf_op jit(solution)/shard_map/ppermute | solution.py:18
  79.4 4.6 %collective-permute-done.5 = bf16[16,64,128]{2,1,0:T(8,128)(2,1)S(1)} collective-permute-done((bf16[16,64,128]{2,1,0:T(8,128)(2,1)S(1)}, bf16[16,64,128]{2,1,0:T(8,128)(2,1)S(1)}, u32[]{:S(2)}, u32[]{:S(2)}) %collective-permute-start.5) | collective-permute-done | bytes 262176 | tf_op jit(solution)/shard_map/ppermute | solution.py:18
  84.3 5.4 %collective-permute-start.7 = (bf16[16,64,128]{2,1,0:T(8,128)(2,1)S(1)}, bf16[16,64,128]{2,1,0:T(8,128)(2,1)S(1)}, u32[]{:S(2)}, u32[]{:S(2)}) collective-permute-start(bf16[16,64,128]{2,1,0:T(8,128)(2,1)S(1)} %fusion.74), channel_id=1, source_target_pairs={{0,16},{4,20},{8,24},{12,28},{1,17},{5,21},{9,25},{13,29},{2,18},{... | collective-permute-start | bytes 786440 | tf_op jit(solution)/shard_map/ppermute | solution.py:18
  89.7 2.4 %collective-permute-start.6 = (f32[16]{0:T(128)S(1)}, f32[16]{0:T(128)S(1)}, u32[]{:S(2)}, u32[]{:S(2)}) collective-permute-start(f32[16]{0:T(128)S(1)} %get-tuple-element.77), channel_id=1, source_target_pairs={{0,8},{4,12},{8,16},{12,20},{16,24},{20,28},{1,9},{5,13},{9,17},{1... | collective-permute-start | bytes 200 | tf_op jit(solution)/shard_map/ppermute | solution.py:18
  92.2 2.0 collective-permute-done.6
  95.3 31.1 %all-gather.6.cloned.1.call-done = bf16[2,768,2048]{2,1,0:T(8,128)(2,1)} async-done(((bf16[2,768,512]{2,1,0:T(8,128)(2,1)}), bf16[2,768,2048]{2,1,0:T(8,128)(2,1)}) %all-gather.6.cloned.1.call-update) | async-done | bytes 6291472 | tf_op jit(solution)/shard_map/all_gather | solution.py:180
  126.4 5.3 %fusion.101 = f32[2,768,256]{2,1,0:T(8,128)S(1)} fusion(bf16[2,768,2048]{2,1,0:T(8,128)(2,1)} %all-gather.6.cloned.1.call-done, bf16[2,2048,256]{2,1,0:T(8,128)(2,1)} %param.42), kind=kOutput, calls=%fused_computation.161 | convolution fusion | flops 1610612736 | bytes 9961472 | tf_op jit(solution)/shard_map/esd,edf->esf/dot_general | solution.py:197
  132.2 2.9 %multiply_convert_fusion = bf16[2,768,256]{2,1,0:T(8,128)(2,1)} fusion(f32[2,768,256]{2,1,0:T(8,128)S(1)} %fusion.101, bf16[2,768,2048]{2,1,0:T(8,128)(2,1)S(1)} %copy-done.33, bf16[2,2048,256]{2,1,0:T(8,128)(2,1)S(1)} %copy-done.35), kind=kOutput, calls=%fused_computation.25 | convolution fusion | flops 1612972032 | bytes 10747904 | tf_op jit(solution)/shard_map/esd,edf->esf/dot_general | solution.py:200
  138.4 2.0 copy.95
  146.3 4.2 %fusion.27 = f32[2,128,16,64]{1,3,2,0:T(8,128)S(1)} fusion(f32[2,128,16,128]{3,1,2,0:T(8,128)S(1)} %bitcast.121, f32[2,16,64,128]{3,2,1,0:T(8,128)S(1)} %copy-done.11, f32[2,128,16]{1,2,0:T(8,128)S(1)} %copy-done.13, f32[16,64,128]{2,1,0:T(8,128)S(1)} %copy-done.9, f32[2,16]{1,0:T(2,128)S(1)} %copy-done.27), kind=kOutput, calls=%fused_computation.37 | convolution fusion | flops 403439616 | bytes 4735104 | tf_op jit(solution)/shard_map/bihn,bhpn->bihp/dot_general | solution.py:184
  151.7 4.2 %fusion.24 = f32[2,128,16,64]{1,3,2,0:T(8,128)S(1)} fusion(f32[2,128,16,64]{1,3,2,0:T(8,128)S(1)} %fusion.27, f32[2,16,128,128]{3,2,1,0:T(8,128)S(1)} %bitcast.119, f32[2,128,16,64]{1,0,3,2:T(2,128)S(1)} %copy-done.6, f32[2,16,128]{2,1,0:T(8,128)S(1)} %copy.85, pred[128,128]{1,0:T(8,128)(4,1)S(1)} %copy-done.12), kind=kOutput, calls=%fused_computation.35 | convolution fusion | flops 405012480 | bytes 5275648 | tf_op jit(solution)/shard_map/bhij,bjhp->bihp/dot_general | solution.py:151
  157.7 3.2 %reshape.140 = f32[256,4,256]{0,2,1:T(8,128)} reshape(f32[2,128,16,64]{1,0,3,2:T(2,128)} %copy.94) | data formatting | bytes 2097152 | tf_op jit(solution)/shard_map/reshape | solution.py:187
  160.9 2.0 multiply_reduce_fusion
  164.4 14.7 %all-gather.10.cloned.1.call-done = bf16[2,768,1024]{2,1,0:T(8,128)(2,1)} async-done(((bf16[2,768,256]{2,1,0:T(8,128)(2,1)}), bf16[2,768,1024]{2,1,0:T(8,128)(2,1)}) %all-gather.10.cloned.1.call-update) | async-done | bytes 3145744 | tf_op jit(solution)/shard_map/all_gather | solution.py:208
  179.0 3.7 %convolution_convert_fusion = bf16[2,768,512]{2,1,0:T(8,128)(2,1)S(1)} fusion(bf16[2,768,1024]{2,1,0:T(8,128)(2,1)} %all-gather.10.cloned.1.call-done, bf16[2,1024,512]{2,1,0:T(8,128)(2,1)S(1)} %copy-done), kind=kOutput, calls=%fused_computation.21 | convolution fusion | flops 1611399168 | bytes 6815744 | tf_op jit(solution)/shard_map/esf,efd->esd/dot_general | solution.py:217
  184.4 4.7 %all-to-all-start = ((bf16[8,192,512]{2,1,0:T(8,128)(2,1)}), bf16[8,192,512]{2,1,0:T(8,128)(2,1)}, u32[]{:S(2)}, u32[]{:S(2)}) async-start(bf16[8,192,512]{2,1,0:T(8,128)(2,1)} %pad_maximum_fusion.1), calls=%async_computation | async-start | bytes 3145728 | tf_op jit(solution)/shard_map/all_to_all | solution.py:224
  189.4 30.9 %all-gather.8.cloned.1.call-done = bf16[256,5120]{0,1:T(8,128)(2,1)} async-done(((bf16[256,1280]{0,1:T(8,128)(2,1)}), bf16[256,5120]{0,1:T(8,128)(2,1)}) %all-gather.8.cloned.1.call-update) | async-done | bytes 2621456 | tf_op jit(solution)/shard_map/all_gather | solution.py:209
  224.2 2.0 convolution_convert_fusion.1
  227.0 2.4 %fusion.47 = f32[256,512]{1,0:T(8,128)S(1)} fusion(bf16[1536,512]{1,0:T(8,128)(2,1)} %bitcast.43, f32[256]{0:T(256)S(1)} %bitcast.151, s32[256]{0:T(256)S(1)} %bitcast.157, f32[256]{0:T(256)S(1)} %bitcast.153, s32[256]{0:T(256)S(1)} %bitcast.159, f32[256]{0:T(256)S(1)} %bitcast.149, s32[256]{0:T(256)S(1)} %bitcast.161, f32[256]{0:T(256)S(1)} %bitcast.147, ...), kind=kOutput, calls=%fused_computation.70 | convolution fusion | flops 407764992 | bytes 2105344 | tf_op jit(solution)/shard_map/dot_general | solution.py:239
  229.5 2.6 %convolution_add_fusion.1 = f32[256,512]{1,0:T(8,128)S(1)} fusion(f32[256,512]{1,0:T(8,128)S(1)} %fusion.47, bf16[1536,512]{1,0:T(8,128)(2,1)} %bitcast.43, f32[256]{0:T(256)S(1)} %bitcast.152, s32[256]{0:T(256)S(1)} %bitcast.158, f32[256]{0:T(256)S(1)} %bitcast.154, s32[256]{0:T(256)S(1)} %bitcast.160, f32[256]{0:T(256)S(1)} %bitcast.150, ...), kind=kOutput, calls=%fused_computation.41 | convolution fusion | flops 408289280 | bytes 2629632 | tf_op jit(solution)/shard_map/dot_general | solution.py:241
  (177 shorter events, 53.4 us)
Async XLA Ops:
  7.2 171.9 %copy-start = (bf16[2,1024,512]{2,1,0:T(8,128)(2,1)S(1)}, bf16[2,1024,512]{2,1,0:T(8,128)(2,1)}, u32[]{:S(2)}) copy-start(bf16[2,1024,512]{2,1,0:T(8,128)(2,1)} %param.44) | copy-start | bytes 6291460
  7.2 8.8 %copy-start.7 = (bf16[256,2048]{1,0:T(8,128)(2,1)S(1)}, bf16[256,2048]{1,0:T(8,128)(2,1)}, u32[]{:S(2)}) copy-start(bf16[256,2048]{1,0:T(8,128)(2,1)} %param.38) | copy-start | bytes 3145732
  7.2 8.2 %copy-start.17 = (s32[256,4]{0,1:T(4,128)S(1)}, s32[256,4]{0,1:T(4,128)}, u32[]{:S(2)}) copy-start(s32[256,4]{0,1:T(4,128)} %param.40) | copy-start | bytes 12292
  7.2 8.8 %copy-start.22 = (f32[2048]{0:T(1024)S(1)}, f32[2048]{0:T(1024)}, u32[]{:S(2)}) copy-start(f32[2048]{0:T(1024)} %param.39) | copy-start | bytes 24580
  7.2 42.7 %all-gather.12.cloned.1.call-start = ((), (), s32[]{:S(2)}) async-start(), calls=%async_computation.4 | async-start | bytes 2433024 | tf_op jit(solution)/shard_map/all_gather | solution.py:133
  10.7 14.2 %collective-permute-start = (bf16[3,2048]{0,1:T(8,128)(2,1)}, bf16[3,2048]{0,1:T(8,128)(2,1)}, u32[]{:S(2)}, u32[]{:S(2)}) collective-permute-start(bf16[3,2048]{0,1:T(8,128)(2,1)} %copy.77), channel_id=1, source_target_pairs={{0,4},{4,8},{8,12},{12,16},{16,20},{20,24},{24,28},{1,5},{5,9},{9,... | collective-permute-start | bytes 36872 | tf_op jit(solution)/shard_map/ppermute | solution.py:18
  16.1 4.4 %copy-start.24 = (f32[4,512]{1,0:T(4,128)S(1)}, f32[4,512]{1,0:T(4,128)}, u32[]{:S(2)}) copy-start(f32[4,512]{1,0:T(4,128)} %param.35) | copy-start | bytes 24580
  16.1 5.0 %copy-start.19 = (f32[4,1024]{1,0:T(4,128)S(1)}, f32[4,1024]{1,0:T(4,128)}, u32[]{:S(2)}) copy-start(f32[4,1024]{1,0:T(4,128)} %param.33) | copy-start | bytes 49156
  18.2 108.2 %all-gather.6.cloned.1.call-start = ((), (), s32[]{:S(2)}) async-start(), calls=%async_computation.1 | async-start | bytes 7864320 | tf_op jit(solution)/shard_map/all_gather | solution.py:180
  38.6 3.0 %copy-start.8 = (f32[2,128,4,128]{3,1,2,0:T(8,128)S(1)}, f32[2,128,4,128]{3,1,2,0:T(8,128)}, u32[]{:S(2)}) copy-start(f32[2,128,4,128]{3,1,2,0:T(8,128)} %copy.89) | copy-start | bytes 1572868
  41.8 3.1 %copy-start.28 = (f32[2,16]{1,0:T(2,128)S(1)}, f32[2,16]{1,0:T(2,128)}, u32[]{:S(2)}) copy-start(f32[2,16]{1,0:T(2,128)} %get-tuple-element.151) | copy-start | bytes 388
  44.9 5.9 %copy-start.29 = (f32[2]{0:T(128)S(1)}, f32[2]{0:T(128)}, u32[]{:S(2)}) copy-start(f32[2]{0:T(128)} %add_convert_fusion) | copy-start | bytes 28
  55.4 8.8 %copy-start.31 = (f32[16]{0:T(128)S(1)}, f32[16]{0:T(128)}, u32[]{:S(2)}) copy-start(f32[16]{0:T(128)} %get-tuple-element.84) | copy-start | bytes 196
  55.4 123.6 %all-gather.10.cloned.1.call-start = ((), (), s32[]{:S(2)}) async-start(), calls=%async_computation.3 | async-start | bytes 3932160 | tf_op jit(solution)/shard_map/all_gather | solution.py:208
  55.5 4.1 %collective-permute-start.1 = (bf16[16,64,128]{2,1,0:T(8,128)(2,1)S(1)}, bf16[16,64,128]{2,1,0:T(8,128)(2,1)S(1)}, u32[]{:S(2)}, u32[]{:S(2)}) collective-permute-start(bf16[16,64,128]{2,1,0:T(8,128)(2,1)S(1)} %convert_element_type.179), channel_id=1, source_target_pairs={{0,4},{4,8},{8,12},{12,16},{16,20},{20,24},{24,28},{1,5},{5,9},{9,... | collective-permute-start | bytes 786440 | tf_op jit(solution)/shard_map/ppermute | solution.py:18
  59.7 13.1 %collective-permute-start.3 = (bf16[16,64,128]{2,1,0:T(8,128)(2,1)S(1)}, bf16[16,64,128]{2,1,0:T(8,128)(2,1)S(1)}, u32[]{:S(2)}, u32[]{:S(2)}) collective-permute-start(bf16[16,64,128]{2,1,0:T(8,128)(2,1)S(1)} %collective-permute-done.1), channel_id=1, source_target_pairs={{0,4},{4,8},{8,12},{12,16},{16,20},{20,24},{24,28},{1,5},{5,9},{9,... | collective-permute-start | bytes 786440 | tf_op jit(solution)/shard_map/ppermute | solution.py:18
  64.2 5.2 %collective-permute-start.2 = (f32[16]{0:T(128)S(1)}, f32[16]{0:T(128)S(1)}, u32[]{:S(2)}, u32[]{:S(2)}) collective-permute-start(f32[16]{0:T(128)S(1)} %copy-done.31), channel_id=1, source_target_pairs={{0,4},{4,8},{8,12},{12,16},{16,20},{20,24},{24,28},{1,5},{5,9},{9,... | collective-permute-start | bytes 200 | tf_op jit(solution)/shard_map/ppermute | solution.py:18
  69.4 3.3 %collective-permute-start.4 = (f32[16]{0:T(128)S(1)}, f32[16]{0:T(128)S(1)}, u32[]{:S(2)}, u32[]{:S(2)}) collective-permute-start(f32[16]{0:T(128)S(1)} %collective-permute-done.2), channel_id=1, source_target_pairs={{0,4},{4,8},{8,12},{12,16},{16,20},{20,24},{24,28},{1,5},{5,9},{9,... | collective-permute-start | bytes 200 | tf_op jit(solution)/shard_map/ppermute | solution.py:18
  72.9 11.1 %collective-permute-start.5 = (bf16[16,64,128]{2,1,0:T(8,128)(2,1)S(1)}, bf16[16,64,128]{2,1,0:T(8,128)(2,1)S(1)}, u32[]{:S(2)}, u32[]{:S(2)}) collective-permute-start(bf16[16,64,128]{2,1,0:T(8,128)(2,1)S(1)} %fusion.72), channel_id=1, source_target_pairs={{0,8},{4,12},{8,16},{12,20},{16,24},{20,28},{1,9},{5,13},{9,17},{1... | collective-permute-start | bytes 786440 | tf_op jit(solution)/shard_map/ppermute | solution.py:18
  84.3 9.9 %collective-permute-start.7 = (bf16[16,64,128]{2,1,0:T(8,128)(2,1)S(1)}, bf16[16,64,128]{2,1,0:T(8,128)(2,1)S(1)}, u32[]{:S(2)}, u32[]{:S(2)}) collective-permute-start(bf16[16,64,128]{2,1,0:T(8,128)(2,1)S(1)} %fusion.74), channel_id=1, source_target_pairs={{0,16},{4,20},{8,24},{12,28},{1,17},{5,21},{9,25},{13,29},{2,18},{... | collective-permute-start | bytes 786440 | tf_op jit(solution)/shard_map/ppermute | solution.py:18
  89.7 4.5 %collective-permute-start.6 = (f32[16]{0:T(128)S(1)}, f32[16]{0:T(128)S(1)}, u32[]{:S(2)}, u32[]{:S(2)}) collective-permute-start(f32[16]{0:T(128)S(1)} %get-tuple-element.77), channel_id=1, source_target_pairs={{0,8},{4,12},{8,16},{12,20},{16,24},{20,28},{1,9},{5,13},{9,17},{1... | collective-permute-start | bytes 200 | tf_op jit(solution)/shard_map/ppermute | solution.py:18
  126.4 5.4 %copy-start.33 = (bf16[2,768,2048]{2,1,0:T(8,128)(2,1)S(1)}, bf16[2,768,2048]{2,1,0:T(8,128)(2,1)}, u32[]{:S(2)}) copy-start(bf16[2,768,2048]{2,1,0:T(8,128)(2,1)} %all-gather.6.cloned.1.call-done) | copy-start | bytes 18874372
  126.4 5.8 %copy-start.35 = (bf16[2,2048,256]{2,1,0:T(8,128)(2,1)S(1)}, bf16[2,2048,256]{2,1,0:T(8,128)(2,1)}, u32[]{:S(2)}) copy-start(bf16[2,2048,256]{2,1,0:T(8,128)(2,1)} %param.43) | copy-start | bytes 6291460
  132.2 3.0 %copy-start.30 = (f32[16]{0:T(128)S(1)}, f32[16]{0:T(128)}, u32[]{:S(2)}) copy-start(f32[16]{0:T(128)} %param.32) | copy-start | bytes 196
  135.1 5.9 %copy-start.4 = (bf16[256,2048]{1,0:T(8,128)(2,1)S(1)}, bf16[256,2048]{1,0:T(8,128)(2,1)}, u32[]{:S(2)}) copy-start(bf16[256,2048]{1,0:T(8,128)(2,1)} %copy-done.3) | copy-start | bytes 3145732
  135.2 85.1 %all-gather.8.cloned.1.call-start = ((), (), s32[]{:S(2)}) async-start(), calls=%async_computation.2 | async-start | bytes 3276800 | tf_op jit(solution)/shard_map/all_gather | solution.py:209
  157.7 3.2 %copy-start.1 = (f32[256,1024]{0,1:T(8,128)S(1)}, f32[256,1024]{0,1:T(8,128)}, u32[]{:S(2)}) copy-start(f32[256,1024]{0,1:T(8,128)} %fusion.71) | copy-start | bytes 3145732
  157.7 3.2 %copy-start.16 = (f32[4,256]{1,0:T(4,128)S(1)}, f32[4,256]{1,0:T(4,128)}, u32[]{:S(2)}) copy-start(f32[4,256]{1,0:T(4,128)} %mul.377) | copy-start | bytes 12292
  184.4 4.8 %copy-start.14 = (f32[4,256]{1,0:T(4,128)S(1)}, f32[4,256]{1,0:T(4,128)}, u32[]{:S(2)}) copy-start(f32[4,256]{1,0:T(4,128)} %get-tuple-element.110) | copy-start | bytes 12292
  184.4 5.0 %copy-start.26 = (f32[256,4]{0,1:T(4,128)S(1)}, f32[256,4]{0,1:T(4,128)}, u32[]{:S(2)}) copy-start(f32[256,4]{0,1:T(4,128)} %param.41) | copy-start | bytes 12292
  184.4 5.0 %copy-start.18 = (s32[256,4]{0,1:T(4,128)S(1)}, s32[256,4]{0,1:T(4,128)}, u32[]{:S(2)}) copy-start(s32[256,4]{0,1:T(4,128)} %param.40) | copy-start | bytes 12292
  184.4 42.6 %all-to-all-start = ((bf16[8,192,512]{2,1,0:T(8,128)(2,1)}), bf16[8,192,512]{2,1,0:T(8,128)(2,1)}, u32[]{:S(2)}, u32[]{:S(2)}) async-start(bf16[8,192,512]{2,1,0:T(8,128)(2,1)} %pad_maximum_fusion.1), calls=%async_computation | async-start | bytes 3145728 | tf_op jit(solution)/shard_map/all_to_all | solution.py:224
  (19 other events, 37.5 us)
Sparse Core Ops, SparseCore 0:
  18.4 31.4 all-gather.11
  55.5 70.8 all-gather.5
  135.3 43.6 all-gather.9
  180.7 39.4 all-gather.7
where the time goes:
time: 241 us; the launch traced here: 240 us
  waiting for transfers between devices  87.8 us (36%)
  matrix products  37.4 us (16%)
  starting transfers between devices  36.9 us (15%)
  local copies, waits for them, and re-layouts  34.6 us (14%)
  other arithmetic  28.6 us (12%)
  between operations  14.4 us (6%)
    ppermute x8, starting transfers between devices, passed_along(): return lax.ppermute(x, axis, pairs)  32 us
    all_gather x1, waiting for transfers between devices, on_device(): column_piece = lax.all_gather(arrived, 'tp', axis=2, tiled=True)  31.1 us
    all_gather x1, waiting for transfers between devices, on_device(): lax.all_gather(jnp.concatenate([mixer_normed, shared_hidden], axis=1), 't...  30.9 us
    all_gather x1, waiting for transfers between devices, on_device(): whole_hidden = lax.all_gather(hidden, 'tp', axis=2, tiled=True)  14.7 us
    ppermute x8, waiting for transfers between devices, passed_along(): return lax.ppermute(x, axis, pairs)  9.39 us
    unnamed x77, local copies, waits for them, and re-layouts  6.78 us
    dot_general x1, matrix products, on_device(): jnp.einsum('esd,edf->esf', column_piece, routed_gate_weight, preferred_el...  5.34 us
  transfers between devices with their start and end apart: 13, of which 10 were waited for; matrix products, arithmetic and copies ran while one was open for 30% of the time, Pallas kernels for 0%

commit v1 on v0

--- a/solution.py
+++ b/solution.py
@@ -177,7 +177,7 @@
             for j in range(local_experts)
         ]
     )
-    column_piece = lax.all_gather(arrived, "tp", axis=2, tiled=True)
+    column_piece = jnp.concatenate(lax.all_gather(arrived, "tp"), axis=2)
     column_piece, incoming = lax.optimization_barrier((column_piece, incoming))
     entering = local_prev + jnp.exp(before_logs)[:, :, None, None] * incoming[None]
     carried_term = (

time: 241 us -> 241 us (level)
  matrix products: 37.4 us -> 33.9 us
  local copies, waits for them, and re-layouts: 34.6 us -> 38.1 us
    reshape x0 -> x1, local copies, waits for them, and re-layouts: none -> 3.9 us  [on_device(): column_piece = jnp.concatenate(lax.all_gather(arrived, 'tp'), axis=2)]
    dot_general x1, matrix products: 5.34 us -> 1.79 us  [on_device(): jnp.einsum('esd,edf->esf', column_piece, routed_gate_weight, preferred_el...]
where the time goes in v1:
time: 241 us; the launch traced here: 240 us
  waiting for transfers between devices  88 us (37%)
  local copies, waits for them, and re-layouts  38.1 us (16%)
  starting transfers between devices  36.8 us (15%)
  matrix products  33.9 us (14%)
  other arithmetic  28.6 us (12%)
  between operations  14.5 us (6%)
    ppermute x8, starting transfers between devices, passed_along(): return lax.ppermute(x, axis, pairs)  32 us
    all_gather x1, waiting for transfers between devices, on_device(): column_piece = jnp.concatenate(lax.all_gather(arrived, 'tp'), axis=2)  31.2 us
    all_gather x1, waiting for transfers between devices, on_device(): lax.all_gather(jnp.concatenate([mixer_normed, shared_hidden], axis=1), 't...  30.9 us
    all_gather x1, waiting for transfers between devices, on_device(): whole_hidden = lax.all_gather(hidden, 'tp', axis=2, tiled=True)  14.7 us
    ppermute x8, waiting for transfers between devices, passed_along(): return lax.ppermute(x, axis, pairs)  9.39 us
    unnamed x77, local copies, waits for them, and re-layouts  6.33 us
  transfers between devices with their start and end apart: 13, of which 10 were waited for; matrix products, arithmetic and copies ran while one was open for 30% of the time, Pallas kernels for 0%

profile of v1, /device:TPU:0, one launch (start us, length us, event | category | flops | bytes accessed | tf_op | source)
XLA Modules:
  0.0 239.8 jit_solution(16747885393225792839)
XLA Ops:
  10.7 3.2 %collective-permute-start = (bf16[3,2048]{0,1:T(8,128)(2,1)}, bf16[3,2048]{0,1:T(8,128)(2,1)}, u32[]{:S(2)}, u32[]{:S(2)}) collective-permute-start(bf16[3,2048]{0,1:T(8,128)(2,1)} %copy.80), channel_id=1, source_target_pairs={{0,4},{4,8},{8,12},{12,16},{16,20},{20,24},{24,28},{1,5},{5,9},{9,... | collective-permute-start | bytes 36872 | tf_op jit(solution)/shard_map/ppermute | solution.py:18
  26.7 3.4 %multiply_convert_fusion.2 = (bf16[256,512]{1,0:T(8,128)(2,1)}, bf16[256,512]{1,0:T(8,128)(2,1)}) fusion(bf16[256,512]{1,0:T(8,128)(2,1)} %param.26, bf16[3,512]{1,0:T(4,128)(2,1)} %copy.84, f32[512]{0:T(512)} %bitcast.149, f32[512]{0:T(512)} %bitcast.150, f32[512]{0:T(512)} %bitcast.148, f32[512]{0:T(512)} %bitcast.147, f32[512]{0:T(512)} %bitcast.153, ...), kind=kLoop, calls=%fused_computation.103 | loop fusion | flops 6553600 | bytes 1071104 | tf_op jit(solution)/shard_map/convert_element_type | solution.py:44
  32.9 2.9 %fusion.71 = f32[256,1024]{0,1:T(8,128)} fusion(f32[1024]{0:T(1024)} %bitcast.142, bf16[256,1024]{0,1:T(8,128)(2,1)S(1)} %copy.81, f32[1024]{0:T(1024)} %bitcast.143, bf16[3,1024]{0,1:T(8,128)(2,1)S(1)} %slice.176, f32[1024]{0:T(1024)} %bitcast.141, f32[1024]{0:T(1024)} %bitcast.140), kind=kLoop, calls=%fused_computation.106 | loop fusion | flops 6815744 | bytes 1595392 | tf_op jit(solution)/shard_map/convert_element_type | solution.py:140
  35.8 2.7 %reshape.138 = f32[2,128,16,64]{1,0,3,2:T(2,128)} reshape(f32[256,1024]{0,1:T(8,128)} %fusion.71) | data formatting | bytes 2097152 | tf_op jit(solution)/shard_map/reshape | solution.py:140
  38.6 3.0 %broadcast_multiply_fusion = (f32[2,128,16,64]{1,0,3,2:T(2,128)S(1)}, f32[2,128,16,64]{1,0,3,2:T(2,128)}) fusion(f32[2,128,16]{1,0,2:T(2,128)S(1)} %copy.91, f32[2,128,16,64]{1,0,3,2:T(2,128)} %reshape.138, f32[2,128,16]{1,0,2:T(2,128)} %mul.326), kind=kLoop, calls=%fused_computation.102 | loop fusion | flops 524288 | bytes 3178496 | tf_op jit(solution)/shard_map/bjhn,bjh,bjhp->bhpn/dot_general | solution.py:156
  41.8 3.1 %fusion.37 = f32[2,16,64,128]{3,2,1,0:T(8,128)} fusion(f32[2,128,16,128]{3,1,2,0:T(8,128)S(1)} %bitcast.125, f32[2,128,16,64]{1,0,3,2:T(2,128)S(1)} %get-tuple-element.78), kind=kOutput, calls=%fused_computation.55 | convolution fusion | flops 402653184 | bytes 4194304 | tf_op jit(solution)/shard_map/bjhn,bjh,bjhp->bhpn/dot_general | solution.py:156
  44.9 4.0 %while.13 = (s32[]{:T(128)}, f32[16,64,128]{2,1,0:T(8,128)S(1)}, f32[2,16,64,128]{3,2,1,0:T(8,128)}, f32[2,16]{1,0:T(2,128)S(1)}, f32[2,16,64,128]{3,2,1,0:T(8,128)}, /*index=5*/s32[]{:T(128)}, s32[]{:T(128)}) while((s32[]{:T(128)}, f32[16,64,128]{2,1,0:T(8,128)S(1)}, f32[2,16,64,128]{3,2,1,0:T(8,128)}, f32[2,16]{1,0:T(2,128)S(1)}, ...), condition=%wide.region_3.4_spmd.clone, body=%wide.region_2.3_spmd.clone.sunk | while | flops 524291 | bytes 2621740 | solution.py:158
  51.3 2.3 fusion.18
  55.5 3.0 %collective-permute-start.1 = (bf16[16,64,128]{2,1,0:T(8,128)(2,1)S(1)}, bf16[16,64,128]{2,1,0:T(8,128)(2,1)S(1)}, u32[]{:S(2)}, u32[]{:S(2)}) collective-permute-start(bf16[16,64,128]{2,1,0:T(8,128)(2,1)S(1)} %convert_element_type.179), channel_id=1, source_target_pairs={{0,4},{4,8},{8,12},{12,16},{16,20},{20,24},{24,28},{1,5},{5,9},{9,... | collective-permute-start | bytes 786440 | tf_op jit(solution)/shard_map/ppermute | solution.py:18
  59.7 4.5 %collective-permute-start.3 = (bf16[16,64,128]{2,1,0:T(8,128)(2,1)S(1)}, bf16[16,64,128]{2,1,0:T(8,128)(2,1)S(1)}, u32[]{:S(2)}, u32[]{:S(2)}) collective-permute-start(bf16[16,64,128]{2,1,0:T(8,128)(2,1)S(1)} %collective-permute-done.1), channel_id=1, source_target_pairs={{0,4},{4,8},{8,12},{12,16},{16,20},{20,24},{24,28},{1,5},{5,9},{9,... | collective-permute-start | bytes 786440 | tf_op jit(solution)/shard_map/ppermute | solution.py:18
  64.2 4.4 %collective-permute-start.2 = (f32[16]{0:T(128)S(1)}, f32[16]{0:T(128)S(1)}, u32[]{:S(2)}, u32[]{:S(2)}) collective-permute-start(f32[16]{0:T(128)S(1)} %copy-done.31), channel_id=1, source_target_pairs={{0,4},{4,8},{8,12},{12,16},{16,20},{20,24},{24,28},{1,5},{5,9},{9,... | collective-permute-start | bytes 200 | tf_op jit(solution)/shard_map/ppermute | solution.py:18
  69.4 2.5 %collective-permute-start.4 = (f32[16]{0:T(128)S(1)}, f32[16]{0:T(128)S(1)}, u32[]{:S(2)}, u32[]{:S(2)}) collective-permute-start(f32[16]{0:T(128)S(1)} %collective-permute-done.2), channel_id=1, source_target_pairs={{0,4},{4,8},{8,12},{12,16},{16,20},{20,24},{24,28},{1,5},{5,9},{9,... | collective-permute-start | bytes 200 | tf_op jit(solution)/shard_map/ppermute | solution.py:18
  72.9 6.5 %collective-permute-start.5 = (bf16[16,64,128]{2,1,0:T(8,128)(2,1)S(1)}, bf16[16,64,128]{2,1,0:T(8,128)(2,1)S(1)}, u32[]{:S(2)}, u32[]{:S(2)}) collective-permute-start(bf16[16,64,128]{2,1,0:T(8,128)(2,1)S(1)} %fusion.72), channel_id=1, source_target_pairs={{0,8},{4,12},{8,16},{12,20},{16,24},{20,28},{1,9},{5,13},{9,17},{1... | collective-permute-start | bytes 786440 | tf_op jit(solution)/shard_map/ppermute | solution.py:18
  79.4 4.6 %collective-permute-done.5 = bf16[16,64,128]{2,1,0:T(8,128)(2,1)S(1)} collective-permute-done((bf16[16,64,128]{2,1,0:T(8,128)(2,1)S(1)}, bf16[16,64,128]{2,1,0:T(8,128)(2,1)S(1)}, u32[]{:S(2)}, u32[]{:S(2)}) %collective-permute-start.5) | collective-permute-done | bytes 262176 | tf_op jit(solution)/shard_map/ppermute | solution.py:18
  84.3 5.4 %collective-permute-start.7 = (bf16[16,64,128]{2,1,0:T(8,128)(2,1)S(1)}, bf16[16,64,128]{2,1,0:T(8,128)(2,1)S(1)}, u32[]{:S(2)}, u32[]{:S(2)}) collective-permute-start(bf16[16,64,128]{2,1,0:T(8,128)(2,1)S(1)} %fusion.74), channel_id=1, source_target_pairs={{0,16},{4,20},{8,24},{12,28},{1,17},{5,21},{9,25},{13,29},{2,18},{... | collective-permute-start | bytes 786440 | tf_op jit(solution)/shard_map/ppermute | solution.py:18
  89.7 2.4 %collective-permute-start.6 = (f32[16]{0:T(128)S(1)}, f32[16]{0:T(128)S(1)}, u32[]{:S(2)}, u32[]{:S(2)}) collective-permute-start(f32[16]{0:T(128)S(1)} %get-tuple-element.77), channel_id=1, source_target_pairs={{0,8},{4,12},{8,16},{12,20},{16,24},{20,28},{1,9},{5,13},{9,17},{1... | collective-permute-start | bytes 200 | tf_op jit(solution)/shard_map/ppermute | solution.py:18
  92.2 2.0 collective-permute-done.6
  95.3 31.2 %all-gather.13.cloned.1.call-done = bf16[8,768,512]{2,1,0:T(8,128)(2,1)} async-done(((bf16[2,768,512]{2,1,0:T(8,128)(2,1)}), bf16[8,768,512]{2,1,0:T(8,128)(2,1)}) %all-gather.13.cloned.1.call-update) | async-done | bytes 6291472 | tf_op jit(solution)/shard_map/all_gather | solution.py:180
  126.5 3.9 %copy.102 = bf16[4,2,96,8,512]{4,3,0,2,1:T(8,128)(2,1)S(1)} copy(bf16[4,2,96,8,512]{4,3,2,1,0:T(8,128)(2,1)} %bitcast.127) | data formatting | bytes 12582912 | tf_op jit(solution)/shard_map/reshape | solution.py:180
  132.3 2.9 %multiply_convert_fusion = bf16[2,768,256]{2,1,0:T(8,128)(2,1)} fusion(f32[2,768,256]{2,1,0:T(8,128)S(1)} %fusion.101, bf16[2,768,2048]{2,1,0:T(8,128)(2,1)S(1)} %bitcast.129, bf16[2,2048,256]{2,1,0:T(8,128)(2,1)S(1)} %copy-done.35), kind=kOutput, calls=%fused_computation.25 | convolution fusion | flops 1612972032 | bytes 10747904 | tf_op jit(solution)/shard_map/esd,edf->esf/dot_general | solution.py:200
  138.4 2.0 copy.99
  146.3 4.2 %fusion.27 = f32[2,128,16,64]{1,3,2,0:T(8,128)S(1)} fusion(f32[2,128,16,128]{3,1,2,0:T(8,128)S(1)} %bitcast.126, f32[2,16,64,128]{3,2,1,0:T(8,128)S(1)} %copy-done.11, f32[2,128,16]{1,2,0:T(8,128)S(1)} %copy-done.13, f32[16,64,128]{2,1,0:T(8,128)S(1)} %copy-done.9, f32[2,16]{1,0:T(2,128)S(1)} %copy-done.27), kind=kOutput, calls=%fused_computation.37 | convolution fusion | flops 403439616 | bytes 4735104 | tf_op jit(solution)/shard_map/bihn,bhpn->bihp/dot_general | solution.py:184
  151.7 4.3 %fusion.24 = f32[2,128,16,64]{1,3,2,0:T(8,128)S(1)} fusion(f32[2,128,16,64]{1,3,2,0:T(8,128)S(1)} %fusion.27, f32[2,16,128,128]{3,2,1,0:T(8,128)S(1)} %bitcast.124, f32[2,128,16,64]{1,0,3,2:T(2,128)S(1)} %copy-done.6, f32[2,16,128]{2,1,0:T(8,128)S(1)} %copy.88, pred[128,128]{1,0:T(8,128)(4,1)S(1)} %copy-done.12), kind=kOutput, calls=%fused_computation.35 | convolution fusion | flops 405012480 | bytes 5275648 | tf_op jit(solution)/shard_map/bhij,bjhp->bihp/dot_general | solution.py:151
  157.8 3.2 %reshape.148 = f32[256,4,256]{0,2,1:T(8,128)} reshape(f32[2,128,16,64]{1,0,3,2:T(2,128)} %copy.98) | data formatting | bytes 2097152 | tf_op jit(solution)/shard_map/reshape | solution.py:187
  161.0 2.0 multiply_reduce_fusion
  164.4 14.7 %all-gather.9.cloned.1.call-done = bf16[2,768,1024]{2,1,0:T(8,128)(2,1)} async-done(((bf16[2,768,256]{2,1,0:T(8,128)(2,1)}), bf16[2,768,1024]{2,1,0:T(8,128)(2,1)}) %all-gather.9.cloned.1.call-update) | async-done | bytes 3145744 | tf_op jit(solution)/shard_map/all_gather | solution.py:208
  179.1 3.7 %convolution_convert_fusion = bf16[2,768,512]{2,1,0:T(8,128)(2,1)S(1)} fusion(bf16[2,768,1024]{2,1,0:T(8,128)(2,1)} %all-gather.9.cloned.1.call-done, bf16[2,1024,512]{2,1,0:T(8,128)(2,1)S(1)} %copy-done), kind=kOutput, calls=%fused_computation.21 | convolution fusion | flops 1611399168 | bytes 6815744 | tf_op jit(solution)/shard_map/esf,efd->esd/dot_general | solution.py:217
  184.4 4.7 %all-to-all-start = ((bf16[8,192,512]{2,1,0:T(8,128)(2,1)}), bf16[8,192,512]{2,1,0:T(8,128)(2,1)}, u32[]{:S(2)}, u32[]{:S(2)}) async-start(bf16[8,192,512]{2,1,0:T(8,128)(2,1)} %pad_maximum_fusion.1), calls=%async_computation | async-start | bytes 3145728 | tf_op jit(solution)/shard_map/all_to_all | solution.py:224
  189.4 30.9 %all-gather.7.cloned.1.call-done = bf16[256,5120]{0,1:T(8,128)(2,1)} async-done(((bf16[256,1280]{0,1:T(8,128)(2,1)}), bf16[256,5120]{0,1:T(8,128)(2,1)}) %all-gather.7.cloned.1.call-update) | async-done | bytes 2621456 | tf_op jit(solution)/shard_map/all_gather | solution.py:209
  224.2 2.0 convolution_convert_fusion.1
  227.1 2.4 %fusion.47 = f32[256,512]{1,0:T(8,128)S(1)} fusion(bf16[1536,512]{1,0:T(8,128)(2,1)} %bitcast.45, f32[256]{0:T(256)S(1)} %bitcast.159, s32[256]{0:T(256)S(1)} %bitcast.165, f32[256]{0:T(256)S(1)} %bitcast.161, s32[256]{0:T(256)S(1)} %bitcast.167, f32[256]{0:T(256)S(1)} %bitcast.157, s32[256]{0:T(256)S(1)} %bitcast.169, f32[256]{0:T(256)S(1)} %bitcast.155, ...), kind=kOutput, calls=%fused_computation.70 | convolution fusion | flops 407764992 | bytes 2105344 | tf_op jit(solution)/shard_map/dot_general | solution.py:239
  229.5 2.6 %convolution_add_fusion.1 = f32[256,512]{1,0:T(8,128)S(1)} fusion(f32[256,512]{1,0:T(8,128)S(1)} %fusion.47, bf16[1536,512]{1,0:T(8,128)(2,1)} %bitcast.45, f32[256]{0:T(256)S(1)} %bitcast.160, s32[256]{0:T(256)S(1)} %bitcast.166, f32[256]{0:T(256)S(1)} %bitcast.162, s32[256]{0:T(256)S(1)} %bitcast.168, f32[256]{0:T(256)S(1)} %bitcast.158, ...), kind=kOutput, calls=%fused_computation.41 | convolution fusion | flops 408289280 | bytes 2629632 | tf_op jit(solution)/shard_map/dot_general | solution.py:241
  (178 shorter events, 54.7 us)
Async XLA Ops:
  7.2 171.9 %copy-start = (bf16[2,1024,512]{2,1,0:T(8,128)(2,1)S(1)}, bf16[2,1024,512]{2,1,0:T(8,128)(2,1)}, u32[]{:S(2)}) copy-start(bf16[2,1024,512]{2,1,0:T(8,128)(2,1)} %param.44) | copy-start | bytes 6291460
  7.2 8.8 %copy-start.7 = (bf16[256,2048]{1,0:T(8,128)(2,1)S(1)}, bf16[256,2048]{1,0:T(8,128)(2,1)}, u32[]{:S(2)}) copy-start(bf16[256,2048]{1,0:T(8,128)(2,1)} %param.38) | copy-start | bytes 3145732
  7.2 8.2 %copy-start.17 = (s32[256,4]{0,1:T(4,128)S(1)}, s32[256,4]{0,1:T(4,128)}, u32[]{:S(2)}) copy-start(s32[256,4]{0,1:T(4,128)} %param.40) | copy-start | bytes 12292
  7.2 8.8 %copy-start.22 = (f32[2048]{0:T(1024)S(1)}, f32[2048]{0:T(1024)}, u32[]{:S(2)}) copy-start(f32[2048]{0:T(1024)} %param.39) | copy-start | bytes 24580
  7.2 42.7 %all-gather.11.cloned.1.call-start = ((), (), s32[]{:S(2)}) async-start(), calls=%async_computation.3 | async-start | bytes 2433024 | tf_op jit(solution)/shard_map/all_gather | solution.py:133
  10.7 14.2 %collective-permute-start = (bf16[3,2048]{0,1:T(8,128)(2,1)}, bf16[3,2048]{0,1:T(8,128)(2,1)}, u32[]{:S(2)}, u32[]{:S(2)}) collective-permute-start(bf16[3,2048]{0,1:T(8,128)(2,1)} %copy.80), channel_id=1, source_target_pairs={{0,4},{4,8},{8,12},{12,16},{16,20},{20,24},{24,28},{1,5},{5,9},{9,... | collective-permute-start | bytes 36872 | tf_op jit(solution)/shard_map/ppermute | solution.py:18
  16.0 2.9 %copy-start.20 = (f32[256,16]{0,1:T(8,128)S(1)}, f32[256,16]{0,1:T(8,128)}, u32[]{:S(2)}) copy-start(f32[256,16]{0,1:T(8,128)} %param.29) | copy-start | bytes 49156
  16.1 4.4 %copy-start.24 = (f32[4,512]{1,0:T(4,128)S(1)}, f32[4,512]{1,0:T(4,128)}, u32[]{:S(2)}) copy-start(f32[4,512]{1,0:T(4,128)} %param.35) | copy-start | bytes 24580
  16.1 5.0 %copy-start.19 = (f32[4,1024]{1,0:T(4,128)S(1)}, f32[4,1024]{1,0:T(4,128)}, u32[]{:S(2)}) copy-start(f32[4,1024]{1,0:T(4,128)} %param.33) | copy-start | bytes 49156
  18.2 108.3 %all-gather.13.cloned.1.call-start = ((), (), s32[]{:S(2)}) async-start(), calls=%async_computation.4 | async-start | bytes 7864320 | tf_op jit(solution)/shard_map/all_gather | solution.py:180
  38.6 3.0 %copy-start.8 = (f32[2,128,4,128]{3,1,2,0:T(8,128)S(1)}, f32[2,128,4,128]{3,1,2,0:T(8,128)}, u32[]{:S(2)}) copy-start(f32[2,128,4,128]{3,1,2,0:T(8,128)} %copy.92) | copy-start | bytes 1572868
  41.8 3.1 %copy-start.28 = (f32[2,16]{1,0:T(2,128)S(1)}, f32[2,16]{1,0:T(2,128)}, u32[]{:S(2)}) copy-start(f32[2,16]{1,0:T(2,128)} %get-tuple-element.151) | copy-start | bytes 388
  44.9 5.9 %copy-start.29 = (f32[2]{0:T(128)S(1)}, f32[2]{0:T(128)}, u32[]{:S(2)}) copy-start(f32[2]{0:T(128)} %add_convert_fusion) | copy-start | bytes 28
  55.4 8.8 %copy-start.31 = (f32[16]{0:T(128)S(1)}, f32[16]{0:T(128)}, u32[]{:S(2)}) copy-start(f32[16]{0:T(128)} %get-tuple-element.84) | copy-start | bytes 196
  55.4 123.7 %all-gather.9.cloned.1.call-start = ((), (), s32[]{:S(2)}) async-start(), calls=%async_computation.2 | async-start | bytes 3932160 | tf_op jit(solution)/shard_map/all_gather | solution.py:208
  55.5 4.1 %collective-permute-start.1 = (bf16[16,64,128]{2,1,0:T(8,128)(2,1)S(1)}, bf16[16,64,128]{2,1,0:T(8,128)(2,1)S(1)}, u32[]{:S(2)}, u32[]{:S(2)}) collective-permute-start(bf16[16,64,128]{2,1,0:T(8,128)(2,1)S(1)} %convert_element_type.179), channel_id=1, source_target_pairs={{0,4},{4,8},{8,12},{12,16},{16,20},{20,24},{24,28},{1,5},{5,9},{9,... | collective-permute-start | bytes 786440 | tf_op jit(solution)/shard_map/ppermute | solution.py:18
  59.7 13.1 %collective-permute-start.3 = (bf16[16,64,128]{2,1,0:T(8,128)(2,1)S(1)}, bf16[16,64,128]{2,1,0:T(8,128)(2,1)S(1)}, u32[]{:S(2)}, u32[]{:S(2)}) collective-permute-start(bf16[16,64,128]{2,1,0:T(8,128)(2,1)S(1)} %collective-permute-done.1), channel_id=1, source_target_pairs={{0,4},{4,8},{8,12},{12,16},{16,20},{20,24},{24,28},{1,5},{5,9},{9,... | collective-permute-start | bytes 786440 | tf_op jit(solution)/shard_map/ppermute | solution.py:18
  64.2 5.2 %collective-permute-start.2 = (f32[16]{0:T(128)S(1)}, f32[16]{0:T(128)S(1)}, u32[]{:S(2)}, u32[]{:S(2)}) collective-permute-start(f32[16]{0:T(128)S(1)} %copy-done.31), channel_id=1, source_target_pairs={{0,4},{4,8},{8,12},{12,16},{16,20},{20,24},{24,28},{1,5},{5,9},{9,... | collective-permute-start | bytes 200 | tf_op jit(solution)/shard_map/ppermute | solution.py:18
  69.4 3.3 %collective-permute-start.4 = (f32[16]{0:T(128)S(1)}, f32[16]{0:T(128)S(1)}, u32[]{:S(2)}, u32[]{:S(2)}) collective-permute-start(f32[16]{0:T(128)S(1)} %collective-permute-done.2), channel_id=1, source_target_pairs={{0,4},{4,8},{8,12},{12,16},{16,20},{20,24},{24,28},{1,5},{5,9},{9,... | collective-permute-start | bytes 200 | tf_op jit(solution)/shard_map/ppermute | solution.py:18
  72.9 11.1 %collective-permute-start.5 = (bf16[16,64,128]{2,1,0:T(8,128)(2,1)S(1)}, bf16[16,64,128]{2,1,0:T(8,128)(2,1)S(1)}, u32[]{:S(2)}, u32[]{:S(2)}) collective-permute-start(bf16[16,64,128]{2,1,0:T(8,128)(2,1)S(1)} %fusion.72), channel_id=1, source_target_pairs={{0,8},{4,12},{8,16},{12,20},{16,24},{20,28},{1,9},{5,13},{9,17},{1... | collective-permute-start | bytes 786440 | tf_op jit(solution)/shard_map/ppermute | solution.py:18
  84.3 9.9 %collective-permute-start.7 = (bf16[16,64,128]{2,1,0:T(8,128)(2,1)S(1)}, bf16[16,64,128]{2,1,0:T(8,128)(2,1)S(1)}, u32[]{:S(2)}, u32[]{:S(2)}) collective-permute-start(bf16[16,64,128]{2,1,0:T(8,128)(2,1)S(1)} %fusion.74), channel_id=1, source_target_pairs={{0,16},{4,20},{8,24},{12,28},{1,17},{5,21},{9,25},{13,29},{2,18},{... | collective-permute-start | bytes 786440 | tf_op jit(solution)/shard_map/ppermute | solution.py:18
  89.7 4.5 %collective-permute-start.6 = (f32[16]{0:T(128)S(1)}, f32[16]{0:T(128)S(1)}, u32[]{:S(2)}, u32[]{:S(2)}) collective-permute-start(f32[16]{0:T(128)S(1)} %get-tuple-element.77), channel_id=1, source_target_pairs={{0,8},{4,12},{8,16},{12,20},{16,24},{20,28},{1,9},{5,13},{9,17},{1... | collective-permute-start | bytes 200 | tf_op jit(solution)/shard_map/ppermute | solution.py:18
  126.5 3.9 %copy-start.34 = (bf16[2,2048,256]{2,1,0:T(8,128)(2,1)S(1)}, bf16[2,2048,256]{2,1,0:T(8,128)(2,1)}, u32[]{:S(2)}) copy-start(bf16[2,2048,256]{2,1,0:T(8,128)(2,1)} %param.42) | copy-start | bytes 6291460
  132.3 3.0 %copy-start.30 = (f32[16]{0:T(128)S(1)}, f32[16]{0:T(128)}, u32[]{:S(2)}) copy-start(f32[16]{0:T(128)} %param.32) | copy-start | bytes 196
  135.2 5.9 %copy-start.4 = (bf16[256,2048]{1,0:T(8,128)(2,1)S(1)}, bf16[256,2048]{1,0:T(8,128)(2,1)}, u32[]{:S(2)}) copy-start(bf16[256,2048]{1,0:T(8,128)(2,1)} %copy-done.3) | copy-start | bytes 3145732
  135.2 85.1 %all-gather.7.cloned.1.call-start = ((), (), s32[]{:S(2)}) async-start(), calls=%async_computation.1 | async-start | bytes 3276800 | tf_op jit(solution)/shard_map/all_gather | solution.py:209
  157.8 3.2 %copy-start.1 = (f32[256,1024]{0,1:T(8,128)S(1)}, f32[256,1024]{0,1:T(8,128)}, u32[]{:S(2)}) copy-start(f32[256,1024]{0,1:T(8,128)} %fusion.71) | copy-start | bytes 3145732
  157.8 3.2 %copy-start.16 = (f32[4,256]{1,0:T(4,128)S(1)}, f32[4,256]{1,0:T(4,128)}, u32[]{:S(2)}) copy-start(f32[4,256]{1,0:T(4,128)} %mul.377) | copy-start | bytes 12292
  184.4 4.7 %copy-start.14 = (f32[4,256]{1,0:T(4,128)S(1)}, f32[4,256]{1,0:T(4,128)}, u32[]{:S(2)}) copy-start(f32[4,256]{1,0:T(4,128)} %get-tuple-element.110) | copy-start | bytes 12292
  184.4 5.0 %copy-start.26 = (f32[256,4]{0,1:T(4,128)S(1)}, f32[256,4]{0,1:T(4,128)}, u32[]{:S(2)}) copy-start(f32[256,4]{0,1:T(4,128)} %param.41) | copy-start | bytes 12292
  184.4 5.0 %copy-start.18 = (s32[256,4]{0,1:T(4,128)S(1)}, s32[256,4]{0,1:T(4,128)}, u32[]{:S(2)}) copy-start(s32[256,4]{0,1:T(4,128)} %param.40) | copy-start | bytes 12292
  184.4 42.6 %all-to-all-start = ((bf16[8,192,512]{2,1,0:T(8,128)(2,1)}), bf16[8,192,512]{2,1,0:T(8,128)(2,1)}, u32[]{:S(2)}, u32[]{:S(2)}) async-start(bf16[8,192,512]{2,1,0:T(8,128)(2,1)} %pad_maximum_fusion.1), calls=%async_computation | async-start | bytes 3145728 | tf_op jit(solution)/shard_map/all_to_all | solution.py:224
  (19 other events, 36.4 us)
Sparse Core Ops, SparseCore 0:
  18.4 31.4 all-gather.10
  55.5 70.9 all-gather.12
  135.4 43.6 all-gather.8
  180.8 39.4 all-gather.6
